TPU v7x, 32 devices: a whole 2x2x4 slice. The times are simulated.
32 devices in a mesh: sp: 4 (over z), tp: 4 (over y, x), dp: 2 (over core).
Axes of the slice: x: 2, y: 2, z: 4, core: 2. Of those that a mesh axis runs over, the one named last changes fastest.
Arguments:
- latent: bfloat16 [4, 4096, 2048], P('dp', 'sp'), may hold values from -6 to 6
- context: bfloat16 [4, 1024, 2048], P('dp', 'sp'), may hold values from -6 to 6
- condition: bfloat16 [4, 2048], P('dp', 'sp'), may hold values from -6 to 6
- ctx_cond: bfloat16 [2048], P('sp'), may hold values from -6 to 6
- norm_gain: float32 [2048], replicated, may hold values from 0.1 to 1.9
- w_shift: bfloat16 [2048, 2048], P('sp', 'tp'), may hold values from -0.125 to 0.125
- w_scale: bfloat16 [2048, 2048], P('sp', 'tp'), may hold values from -0.125 to 0.125
- w_gate: bfloat16 [2048, 2048], P('sp', 'tp'), may hold values from -0.125 to 0.125
- w_query: bfloat16 [2048, 1024], P(None, 'tp'), may hold values from -0.125 to 0.125
- w_key: bfloat16 [2048, 256], P(None, 'tp'), may hold values from -0.125 to 0.125
- w_value: bfloat16 [2048, 256], P(None, 'tp'), may hold values from -0.125 to 0.125
- w_out: bfloat16 [1024, 2048], P('tp'), may hold values from -4 to 4
- sink_logit: float32 [16], P('tp'), may hold values from 4 to 7
- ctx_lift: float32 [16], P('tp'), may hold values from -4 to 220
Outputs:
- mixed: bfloat16 [4, 4096, 2048], P('dp', ('sp', 'tp'))
All inputs are finite; a program needn't handle non-finite values.
Results may differ from a plain program's by a relative error of at most 0.012.
Values may be sent and summed in bfloat16 or wider, within the bound.
A program may use at most 128 MiB of HBM per device.

v0:
```python
import jax
import jax.numpy as jnp
from jax import lax
from jax.sharding import PartitionSpec as P

HEAD = 64
WINDOW = 128
GRID_COLS = 64
epsilon = 1e-06
rope_base = 10000.0
masked_value = -1e30


def with_halo(cells, sides, width):
    for axis, dim in sides:
        count = lax.axis_size(axis)
        ends = count - 1
        head = lax.slice_in_dim(cells, 0, width, axis=dim)
        tail = lax.slice_in_dim(cells, cells.shape[dim] - width, cells.shape[dim], axis=dim)
        cells = jnp.concatenate(
            [
                lax.ppermute(tail, axis, [(i, (i + 1) % count) for i in range(ends)]),
                cells,
                lax.ppermute(head, axis, [((i + 1) % count, i) for i in range(ends)]),
            ],
            axis=dim,
        )
    return cells


def modulated(inputs, norm_gain, shift_vec, scale_vec):
    widened = inputs.astype(jnp.float32)
    inverse = lax.rsqrt(jnp.mean(widened * widened, axis=-1, keepdims=True) + epsilon)
    return (widened * inverse * norm_gain * (1.0 + scale_vec) + shift_vec).astype(jnp.bfloat16)


def rotate_half(half_part, angles):
    first_half, second = jnp.split(half_part, 2, axis=-1)
    cosine = jnp.cos(angles)[:, None, :]
    sine_part = jnp.sin(angles)[:, None, :]
    return jnp.concatenate(
        [first_half * cosine - second * sine_part, first_half * sine_part + second * cosine],
        axis=-1,
    )


def rotate(inputs, positions):
    quarter = inputs.shape[-1] // 4
    frequency = rope_base ** (-jnp.arange(quarter, dtype=jnp.float32) / quarter)
    row_angle = (positions // GRID_COLS).astype(jnp.float32)[:, None] * frequency
    col_angle = (positions % GRID_COLS).astype(jnp.float32)[:, None] * frequency
    half_size = 2 * quarter
    return jnp.concatenate(
        [
            rotate_half(inputs[..., :half_size], row_angle),
            rotate_half(inputs[..., half_size:], col_angle),
        ],
        axis=-1,
    )


def shards(
    latent,
    context,
    condition,
    ctx_cond,
    norm_gain,
    w_shift,
    w_scale,
    w_gate,
    w_query,
    w_key,
    w_value,
    w_out,
    sink_logit,
    ctx_lift,
):
    samples, tokens, model_width = latent.shape
    head_size = HEAD
    sp_count = lax.axis_size("sp")
    cond_rows = jnp.concatenate([condition, ctx_cond[None, :]], axis=0)
    active = jax.nn.silu(cond_rows.astype(jnp.float32)).astype(jnp.bfloat16)
    shift_part, scale_part, gate_part = lax.psum(
        (
            jnp.dot(active, w_shift, preferred_element_type=jnp.float32),
            jnp.dot(active, w_scale, preferred_element_type=jnp.float32),
            jnp.dot(active, w_gate, preferred_element_type=jnp.float32),
        ),
        "sp",
    )
    shift_vec, scale_vec, gate_vec = (
        lax.all_gather(shift_part, "tp", axis=1, tiled=True),
        lax.all_gather(scale_part, "tp", axis=1, tiled=True),
        lax.all_gather(gate_part, "tp", axis=1, tiled=True),
    )
    hidden = modulated(
        latent, norm_gain, shift_vec[:samples, None, :], scale_vec[:samples, None, :]
    )
    offset_row = lax.axis_index("sp") * tokens
    positions = offset_row + jnp.arange(tokens, dtype=jnp.int32)
    query_heads = w_query.shape[1] // head_size
    key_heads = w_key.shape[1] // head_size
    group_size = query_heads // key_heads
    keyed = key_heads * head_size
    queries = rotate(
        jnp.einsum("snd,dc->snc", hidden, w_query, preferred_element_type=jnp.float32).reshape(
            samples, tokens, query_heads, head_size
        ),
        positions,
    ).astype(jnp.bfloat16)
    key_rows = rotate(
        jnp.einsum("snd,dc->snc", hidden, w_key, preferred_element_type=jnp.float32).reshape(
            samples, tokens, key_heads, head_size
        ),
        positions,
    ).astype(jnp.bfloat16)
    values = jnp.einsum("snd,dc->snc", hidden, w_value, preferred_element_type=jnp.float32).astype(
        jnp.bfloat16
    )
    local_pairs = jnp.concatenate([key_rows.reshape(samples, tokens, keyed), values], axis=-1)
    extended = with_halo(local_pairs, (("sp", 1),), WINDOW)
    ctx_hidden = modulated(context, norm_gain, shift_vec[samples], scale_vec[samples])
    ctx_keys = jnp.einsum(
        "snd,dc->snc", ctx_hidden, w_key, preferred_element_type=jnp.float32
    ).astype(jnp.bfloat16)
    ctx_values = jnp.einsum(
        "snd,dc->snc", ctx_hidden, w_value, preferred_element_type=jnp.float32
    ).astype(jnp.bfloat16)
    context_pairs = lax.all_gather(
        jnp.concatenate([ctx_keys, ctx_values], axis=-1), "sp", axis=1, tiled=True
    )
    block_rows = min(512, tokens)
    blocks = tokens // block_rows
    span_rows = block_rows + 2 * WINDOW
    latent_len = tokens * sp_count
    lift_rows = ctx_lift.reshape(key_heads, group_size, 1, 1)
    sink_rows = sink_logit.reshape(key_heads, group_size, 1, 1)
    factor = head_size ** (-0.5)

    def attend(step_id):
        sample = step_id // blocks
        row_start = step_id % blocks * block_rows
        q_rows = lax.dynamic_slice_in_dim(
            lax.dynamic_index_in_dim(queries, sample, 0, keepdims=False), row_start, block_rows, 0
        )
        q_rows = q_rows.reshape(block_rows, key_heads, group_size, head_size)
        pair_rows = lax.dynamic_slice_in_dim(
            lax.dynamic_index_in_dim(extended, sample, 0, keepdims=False), row_start, span_rows, 0
        )
        near_keys = pair_rows[:, :keyed].reshape(span_rows, key_heads, head_size)
        near_values = pair_rows[:, keyed:].reshape(span_rows, key_heads, head_size)
        ctx_rows = lax.dynamic_index_in_dim(context_pairs, sample, 0, keepdims=False)
        far_keys = ctx_rows[:, :keyed].reshape(-1, key_heads, head_size)
        far_values = ctx_rows[:, keyed:].reshape(-1, key_heads, head_size)
        query_pos = offset_row + row_start + jnp.arange(block_rows, dtype=jnp.int32)
        key_pos = offset_row + row_start - WINDOW + jnp.arange(span_rows, dtype=jnp.int32)
        inside = (
            (key_pos[None, :] >= 0)
            & (key_pos[None, :] < latent_len)
            & (jnp.abs(query_pos[:, None] - key_pos[None, :]) <= WINDOW)
        )
        near_scores = (
            jnp.einsum("qgrd,kgd->grqk", q_rows, near_keys, preferred_element_type=jnp.float32)
            * factor
        )
        near_scores = jnp.where(inside[None, None], near_scores, masked_value)
        far_scores = (
            jnp.einsum("qgrd,kgd->grqk", q_rows, far_keys, preferred_element_type=jnp.float32)
            * factor
            + lift_rows
        )
        row_max = jnp.maximum(
            jnp.maximum(near_scores.max(-1, keepdims=True), far_scores.max(-1, keepdims=True)),
            sink_rows,
        )
        near_exp = jnp.exp(near_scores - row_max)
        far_exp = jnp.exp(far_scores - row_max)
        normaliser = (
            near_exp.sum(-1, keepdims=True)
            + far_exp.sum(-1, keepdims=True)
            + jnp.exp(sink_rows - row_max)
        )
        outcome = jnp.einsum(
            "grqk,kgd->qgrd",
            (near_exp / normaliser).astype(jnp.bfloat16),
            near_values,
            preferred_element_type=jnp.float32,
        )
        outcome = outcome + jnp.einsum(
            "grqk,kgd->qgrd",
            (far_exp / normaliser).astype(jnp.bfloat16),
            far_values,
            preferred_element_type=jnp.float32,
        )
        return outcome.astype(jnp.bfloat16).reshape(block_rows, query_heads * head_size)

    attended = lax.map(attend, jnp.arange(samples * blocks, dtype=jnp.int32)).reshape(
        samples, tokens, query_heads * head_size
    )
    by_rows = lax.all_to_all(attended, "tp", split_axis=1, concat_axis=2, tiled=True)
    projected = jnp.einsum(
        "snc,cd->snd",
        by_rows,
        lax.all_gather(w_out, "tp", axis=0, tiled=True),
        preferred_element_type=jnp.float32,
    )
    return (gate_vec[:samples, None, :] * projected).astype(jnp.bfloat16)


def solution(mesh):
    return jax.shard_map(
        shards,
        mesh=mesh,
        in_specs=(
            P("dp", "sp", None),
            P("dp", "sp", None),
            P("dp", "sp"),
            P("sp"),
            P(),
            P("sp", "tp"),
            P("sp", "tp"),
            P("sp", "tp"),
            P(None, "tp"),
            P(None, "tp"),
            P(None, "tp"),
            P("tp", None),
            P("tp"),
            P("tp"),
        ),
        out_specs=P("dp", ("sp", "tp"), None),
        check_vma=False,
    )
```

profile of v0, /device:TPU:0, one launch (start us, length us, event | category | flops | bytes accessed | tf_op | source)
XLA Modules:
  0.0 226.5 jit_solution(14336475768110559586)
XLA Ops:
  11.1 21.3 %all-reduce = (f32[3,512]{1,0:T(4,128)S(1)}, f32[3,512]{1,0:T(4,128)S(1)}, f32[3,512]{1,0:T(4,128)}) all-reduce(f32[3,512]{1,0:T(4,128)S(1)} %fusion.70, f32[3,512]{1,0:T(4,128)S(1)} %fusion.72, f32[3,512]{1,0:T(4,128)S(1)} %fusion.74), channel_id=1, replica_groups=mesh['sp'=4,'tp'=4,'dp'=2] {'sp'}, use_global_device_ids=true, to_apply=%region_3.4 | all-reduce | flops 4608 | bytes 36864 | tf_op jit(solution)/shard_map/psum | solution.py:83
  32.3 8.2 %all_gather.17 = f32[3,2048]{1,0:T(4,128)S(1)} all-gather(f32[3,512]{1,0:T(4,128)S(1)} %get-tuple-element.178), channel_id=1, replica_groups=mesh['sp'=4,'tp'=4,'dp'=2] {'tp'}, dimensions={1}, use_global_device_ids=true | all-gather | bytes 30720 | tf_op jit(solution)/shard_map/all_gather | solution.py:92
  40.5 8.2 %all_gather.16 = f32[3,2048]{1,0:T(4,128)S(1)} all-gather(f32[3,512]{1,0:T(4,128)S(1)} %get-tuple-element.179), channel_id=1, replica_groups=mesh['sp'=4,'tp'=4,'dp'=2] {'tp'}, dimensions={1}, use_global_device_ids=true | all-gather | bytes 30720 | tf_op jit(solution)/shard_map/all_gather | solution.py:93
  48.7 5.1 %fusion.26 = f32[2,1024]{1,0:T(2,128)S(1)} fusion(bf16[2,1024,2048]{2,1,0:T(8,128)(2,1)} %param.16), kind=kLoop, calls=%fused_computation.44 | loop fusion | flops 12580864 | bytes 8396800 | tf_op jit(solution)/shard_map/reduce_sum | solution.py:33
  54.4 6.0 %convolution_bitcast_fusion = f32[2,1024,1,64]{1,3,0,2:T(8,128)S(1)} fusion(bf16[2,1024,2048]{2,1,0:T(8,128)(2,1)} %param.16, f32[2,2048]{1,0:T(2,128)S(1)} %slice.74, f32[2,2048]{1,0:T(2,128)S(1)} %slice_add_fusion, f32[2048]{0:T(1024)S(1)} %copy-done.6, f32[2,1024]{1,0:T(2,128)S(1)} %add_rsqrt_fusion, bf16[2048,64]{0,1:T(8,128)(2,1)S(1)} %copy-done.5), kind=kOutput, calls=%fused_computation.59 | convolution fusion | flops 562036736 | bytes 9224192 | tf_op jit(solution)/shard_map/snd,dc->snc/dot_general | solution.py:112
  60.5 6.9 %fusion.40 = bf16[2,1024,128]{1,2,0:T(8,128)(2,1)S(1)} fusion(bf16[2,1024,128]{1,2,0:T(8,128)(2,1)S(1)} %fusion.59, bf16[2,1024,2048]{2,1,0:T(8,128)(2,1)} %param.16, f32[2,2048]{1,0:T(2,128)S(1)} %slice.74, f32[2,2048]{1,0:T(2,128)S(1)} %slice_add_fusion, f32[2048]{0:T(1024)S(1)} %copy-done.6, f32[2,1024]{1,0:T(2,128)S(1)} %add_rsqrt_fusion, ...), kind=kOutput, calls=%fused_computation.61 | convolution fusion | flops 562167808 | bytes 8962048 | tf_op jit(solution)/shard_map/snd,dc->snc/dot_general | solution.py:117
  70.4 2.1 fusion.31
  72.4 2.6 %convolution_convert_fusion.1 = bf16[2,256,64]{1,2,0:T(8,128)(2,1)S(1)} fusion(bf16[2,256,2048]{2,1,0:T(8,128)(2,1)} %param.17, f32[2048]{0:T(1024)S(1)} %bitcast.202, f32[2048]{0:T(1024)S(1)} %bitcast.200, f32[2048]{0:T(1024)S(1)} %copy-done.6, f32[2,256]{1,0:T(2,128)S(1)} %add_rsqrt_fusion.1, bf16[2048,64]{0,1:T(8,128)(2,1)S(1)} %copy-done.4), kind=kOutput, calls=%fused_computation.62 | convolution fusion | flops 140541952 | bytes 2451456 | tf_op jit(solution)/shard_map/snd,dc->snc/dot_general | solution.py:126
  75.1 2.6 %convolution_convert_fusion.2 = bf16[2,256,64]{1,2,0:T(8,128)(2,1)S(1)} fusion(bf16[2,256,2048]{2,1,0:T(8,128)(2,1)} %param.17, f32[2048]{0:T(1024)S(1)} %bitcast.203, f32[2048]{0:T(1024)S(1)} %bitcast.201, f32[2048]{0:T(1024)S(1)} %copy-done.6, f32[2,256]{1,0:T(2,128)S(1)} %add_rsqrt_fusion.1, bf16[2048,64]{0,1:T(8,128)(2,1)S(1)} %copy-done.5), kind=kOutput, calls=%fused_computation.63 | convolution fusion | flops 140541952 | bytes 2451456 | tf_op jit(solution)/shard_map/snd,dc->snc/dot_general | solution.py:123
  77.7 6.7 %fusion.43 = f32[2,1024,256]{1,2,0:T(8,128)S(1)} fusion(bf16[2048,256]{1,0:T(8,128)(2,1)S(1)} %copy-done, bf16[2,1024,2048]{2,1,0:T(8,128)(2,1)} %param.16, f32[2,2048]{1,0:T(2,128)S(1)} %slice.74, f32[2,2048]{1,0:T(2,128)S(1)} %slice_add_fusion, f32[2048]{0:T(1024)S(1)} %copy-done.6, f32[2,1024]{1,0:T(2,128)S(1)} %add_rsqrt_fusion), kind=kOutput, calls=%fused_computation.65 | convolution fusion | flops 2172649472 | bytes 11583488 | tf_op jit(solution)/shard_map/snd,dc->snc/dot_general | solution.py:106
  84.8 15.8 %all_gather.18 = bf16[2,1024,128]{1,2,0:T(8,128)(2,1)S(1)} all-gather(bf16[2,256,128]{1,2,0:T(8,128)(2,1)S(1)} %pad_maximum_fusion.2), channel_id=1, replica_groups=mesh['sp'=4,'tp'=4,'dp'=2] {'sp'}, dimensions={1}, use_global_device_ids=true | all-gather | bytes 655360 | tf_op jit(solution)/shard_map/all_gather | solution.py:129
  102.2 91.8 %while.13 = (s32[]{:T(128)}, bf16[4,512,256]{2,1,0:T(8,128)(2,1)}, s32[4]{0:T(128)}, bf16[2,1280,128]{1,2,0:T(8,128)(2,1)}, s32[]{:T(128)}, /*index=5*/bf16[2,10...) while((s32[]{:T(128)}, bf16[4,512,256]{2,1,0:T(8,128)(2,1)}, ...), condition=%wide.region_10.11_spmd, body=%wide.region_5.10_spmd.sunk | while | flops 985405696 | bytes 75191968 | solution.py:197
  105.8 4.6 %bitcast_reduce_fusion.2 = (f32[4,512]{1,0:T(4,128)S(1)}, f32[1024,512,4]{1,0,2:T(8,128)}) fusion(f32[4]{0:T(128)S(1)} %bitcast.194, bf16[2,1024,4,64]{1,3,2,0:T(8,128)(2,1)S(1)} %get-tuple-element.303, s32[]{:T(128)S(6)} %select_n.121, s32[]{:T(128)S(6)} %select_n.124, bf16[1024,128]{0,1:T(8,128)(2,1)S(1)} %dynamic-slice_bitcast_fusion.4), kind=kOutput, calls=%fused_computation.1.clone.1 | convolution fusion | flops 274724864 | bytes 8790536 | tf_op jit(solution)/shard_map/while/body/eval_jaxpr/qgrd,kgd->grqk/dot_general | solution.py:168
  113.4 5.2 %fusion.94 = f32[4,512]{1,0:T(4,128)S(1)} fusion(f32[1024,512,4]{1,0,2:T(8,128)} %get-tuple-element.260, f32[4,512]{1,0:T(4,128)S(1)} %maximum_maximum_fusion.2, f32[4]{0:T(128)S(1)} %bitcast.195), kind=kLoop, calls=%fused_computation.5.clone.1 | loop fusion | flops 8386560 | bytes 8405008 | tf_op jit(solution)/shard_map/while/body/eval_jaxpr/reduce_sum | solution.py:180
  120.2 2.1 fusion.95
  122.3 2.0 fusion.96
  128.8 4.6 %bitcast_reduce_fusion.2 = (f32[4,512]{1,0:T(4,128)S(1)}, f32[1024,512,4]{1,0,2:T(8,128)}) fusion(f32[4]{0:T(128)S(1)} %bitcast.194, bf16[2,1024,4,64]{1,3,2,0:T(8,128)(2,1)S(1)} %get-tuple-element.303, s32[]{:T(128)S(6)} %select_n.121, s32[]{:T(128)S(6)} %select_n.124, bf16[1024,128]{0,1:T(8,128)(2,1)S(1)} %dynamic-slice_bitcast_fusion.4), kind=kOutput, calls=%fused_computation.1.clone.1 | convolution fusion | flops 274724864 | bytes 8790536 | tf_op jit(solution)/shard_map/while/body/eval_jaxpr/qgrd,kgd->grqk/dot_general | solution.py:168
  136.4 5.2 %fusion.94 = f32[4,512]{1,0:T(4,128)S(1)} fusion(f32[1024,512,4]{1,0,2:T(8,128)} %get-tuple-element.260, f32[4,512]{1,0:T(4,128)S(1)} %maximum_maximum_fusion.2, f32[4]{0:T(128)S(1)} %bitcast.195), kind=kLoop, calls=%fused_computation.5.clone.1 | loop fusion | flops 8386560 | bytes 8405008 | tf_op jit(solution)/shard_map/while/body/eval_jaxpr/reduce_sum | solution.py:180
  143.1 2.1 fusion.95
  145.2 2.0 fusion.96
  151.7 4.6 %bitcast_reduce_fusion.2 = (f32[4,512]{1,0:T(4,128)S(1)}, f32[1024,512,4]{1,0,2:T(8,128)}) fusion(f32[4]{0:T(128)S(1)} %bitcast.194, bf16[2,1024,4,64]{1,3,2,0:T(8,128)(2,1)S(1)} %get-tuple-element.303, s32[]{:T(128)S(6)} %select_n.121, s32[]{:T(128)S(6)} %select_n.124, bf16[1024,128]{0,1:T(8,128)(2,1)S(1)} %dynamic-slice_bitcast_fusion.4), kind=kOutput, calls=%fused_computation.1.clone.1 | convolution fusion | flops 274724864 | bytes 8790536 | tf_op jit(solution)/shard_map/while/body/eval_jaxpr/qgrd,kgd->grqk/dot_general | solution.py:168
  159.3 5.2 %fusion.94 = f32[4,512]{1,0:T(4,128)S(1)} fusion(f32[1024,512,4]{1,0,2:T(8,128)} %get-tuple-element.260, f32[4,512]{1,0:T(4,128)S(1)} %maximum_maximum_fusion.2, f32[4]{0:T(128)S(1)} %bitcast.195), kind=kLoop, calls=%fused_computation.5.clone.1 | loop fusion | flops 8386560 | bytes 8405008 | tf_op jit(solution)/shard_map/while/body/eval_jaxpr/reduce_sum | solution.py:180
  166.0 2.1 fusion.95
  168.2 2.0 fusion.96
  174.6 4.6 %bitcast_reduce_fusion.2 = (f32[4,512]{1,0:T(4,128)S(1)}, f32[1024,512,4]{1,0,2:T(8,128)}) fusion(f32[4]{0:T(128)S(1)} %bitcast.194, bf16[2,1024,4,64]{1,3,2,0:T(8,128)(2,1)S(1)} %get-tuple-element.303, s32[]{:T(128)S(6)} %select_n.121, s32[]{:T(128)S(6)} %select_n.124, bf16[1024,128]{0,1:T(8,128)(2,1)S(1)} %dynamic-slice_bitcast_fusion.4), kind=kOutput, calls=%fused_computation.1.clone.1 | convolution fusion | flops 274724864 | bytes 8790536 | tf_op jit(solution)/shard_map/while/body/eval_jaxpr/qgrd,kgd->grqk/dot_general | solution.py:168
  182.2 5.2 %fusion.94 = f32[4,512]{1,0:T(4,128)S(1)} fusion(f32[1024,512,4]{1,0,2:T(8,128)} %get-tuple-element.260, f32[4,512]{1,0:T(4,128)S(1)} %maximum_maximum_fusion.2, f32[4]{0:T(128)S(1)} %bitcast.195), kind=kLoop, calls=%fused_computation.5.clone.1 | loop fusion | flops 8386560 | bytes 8405008 | tf_op jit(solution)/shard_map/while/body/eval_jaxpr/reduce_sum | solution.py:180
  189.0 2.1 fusion.95
  191.1 2.0 fusion.96
  194.0 3.3 %copy.27 = bf16[2,1024,256]{2,0,1:T(2,128)(2,1)} copy(bf16[2,1024,256]{2,1,0:T(8,128)(2,1)} %bitcast.191) | data formatting | bytes 2097152 | tf_op jit(solution)/shard_map/reshape | solution.py:197
  197.3 3.5 %all-to-all-start = ((bf16[2,1024,256]{2,0,1:T(2,128)(2,1)}), bf16[2,1024,256]{2,0,1:T(2,128)(2,1)S(1)}, u32[]{:S(2)}, u32[]{:S(2)}) async-start(bf16[2,1024,256]{2,0,1:T(2,128)(2,1)} %copy.27), calls=%async_computation | async-start | bytes 2097152 | tf_op jit(solution)/shard_map/all_to_all | solution.py:200
  200.8 12.7 %all_gather.15 = f32[3,2048]{1,0:T(4,128)S(1)} all-gather(f32[3,512]{1,0:T(4,128)S(1)} %copy-done.3), channel_id=1, replica_groups=mesh['sp'=4,'tp'=4,'dp'=2] {'tp'}, dimensions={1}, use_global_device_ids=true | all-gather | bytes 30720 | tf_op jit(solution)/shard_map/all_gather | solution.py:94
  213.8 5.8 %multiply_convert_fusion = bf16[2,256,2048]{2,1,0:T(8,128)(2,1)} fusion(bf16[2,256,1024]{2,1,0:T(8,128)(2,1)S(1)} %bitcast.192, bf16[1024,2048]{1,0:T(8,128)(2,1)} %all-gather.2.cloned.1.call-done, f32[2,2048]{1,0:T(2,128)S(1)} %slice.72), kind=kOutput, calls=%fused_computation.58 | convolution fusion | flops 2149580800 | bytes 7356416 | tf_op jit(solution)/shard_map/snc,cd->snd/dot_general | solution.py:201
  (121 shorter events, 36.7 us)
Async XLA Ops:
  6.5 71.2 %copy-start = (bf16[2048,256]{1,0:T(8,128)(2,1)S(1)}, bf16[2048,256]{1,0:T(8,128)(2,1)}, u32[]{:S(2)}) copy-start(bf16[2048,256]{1,0:T(8,128)(2,1)} %param.24) | copy-start | bytes 3145732
  6.5 47.8 %copy-start.6 = (f32[2048]{0:T(1024)S(1)}, f32[2048]{0:T(1024)}, u32[]{:S(2)}) copy-start(f32[2048]{0:T(1024)} %param.20) | copy-start | bytes 24580
  6.5 47.8 %copy-start.5 = (bf16[2048,64]{0,1:T(8,128)(2,1)S(1)}, bf16[2048,64]{0,1:T(8,128)(2,1)}, u32[]{:S(2)}) copy-start(bf16[2048,64]{0,1:T(8,128)(2,1)} %param.25) | copy-start | bytes 786436
  6.5 207.2 %all-gather.2.cloned.1.call-start = ((), (), s32[]{:S(2)}) async-start(), calls=%async_computation.1 | async-start | bytes 5242880 | tf_op jit(solution)/shard_map/all_gather | solution.py:204
  54.4 6.1 %copy-start.4 = (bf16[2048,64]{0,1:T(8,128)(2,1)S(1)}, bf16[2048,64]{0,1:T(8,128)(2,1)}, u32[]{:S(2)}) copy-start(bf16[2048,64]{0,1:T(8,128)(2,1)} %param.26) | copy-start | bytes 786436
  67.5 33.2 %collective-permute-start = (bf16[2,128,128]{1,2,0:T(8,128)(2,1)S(1)}, bf16[2,128,128]{1,2,0:T(8,128)(2,1)S(1)}, u32[]{:S(2)}, u32[]{:S(2)}) collective-permute-start(bf16[2,128,128]{1,2,0:T(8,128)(2,1)S(1)} %get-tuple-element.191), channel_id=1, source_target_pairs={{0,8},{8,16},{16,24},{1,9},{9,17},{17,25},{2,10},{10,18},{18,26},{... | collective-permute-start | bytes 196616 | tf_op jit(solution)/shard_map/ppermute | solution.py:22
  68.8 31.9 %collective-permute-start.1 = (bf16[2,128,128]{1,2,0:T(8,128)(2,1)S(1)}, bf16[2,128,128]{1,2,0:T(8,128)(2,1)S(1)}, u32[]{:S(2)}, u32[]{:S(2)}) collective-permute-start(bf16[2,128,128]{1,2,0:T(8,128)(2,1)S(1)} %get-tuple-element.192), channel_id=1, source_target_pairs={{8,0},{16,8},{24,16},{9,1},{17,9},{25,17},{10,2},{18,10},{26,18},{... | collective-permute-start | bytes 196616 | tf_op jit(solution)/shard_map/ppermute | solution.py:24
  84.4 17.8 %copy-start.1 = (f32[4]{0:T(128)S(1)}, f32[4]{0:T(128)}, u32[]{:S(2)}) copy-start(f32[4]{0:T(128)} %param.29) | copy-start | bytes 52
  84.4 17.8 %copy-start.2 = (f32[4]{0:T(128)S(1)}, f32[4]{0:T(128)}, u32[]{:S(2)}) copy-start(f32[4]{0:T(128)} %param.28) | copy-start | bytes 52
  102.2 98.6 %copy-start.3 = (f32[3,512]{1,0:T(4,128)S(1)}, f32[3,512]{1,0:T(4,128)}, u32[]{:S(2)}) copy-start(f32[3,512]{1,0:T(4,128)} %get-tuple-element.180) | copy-start | bytes 18436
  113.4 6.7 %slice-start = ((s8[8388608]{0:T(1024)(128)(4,1)}), s8[4194304]{0:T(1024)(128)(4,1)S(1)}, s32[]{:S(2)}) async-start(s8[8388608]{0:T(1024)(128)(4,1)} %bitcast.186), calls=%async_computation.2 | async-start | bytes 8388608 | tf_op jit(solution)/shard_map/while
  113.4 6.7 %slice-start.1 = ((s8[8388608]{0:T(1024)(128)(4,1)}), s8[4194304]{0:T(1024)(128)(4,1)S(1)}, s32[]{:S(2)}) async-start(s8[8388608]{0:T(1024)(128)(4,1)} %bitcast.186), calls=%async_computation.3 | async-start | bytes 8388608 | tf_op jit(solution)/shard_map/while
  136.4 6.7 %slice-start = ((s8[8388608]{0:T(1024)(128)(4,1)}), s8[4194304]{0:T(1024)(128)(4,1)S(1)}, s32[]{:S(2)}) async-start(s8[8388608]{0:T(1024)(128)(4,1)} %bitcast.186), calls=%async_computation.2 | async-start | bytes 8388608 | tf_op jit(solution)/shard_map/while
  136.4 6.7 %slice-start.1 = ((s8[8388608]{0:T(1024)(128)(4,1)}), s8[4194304]{0:T(1024)(128)(4,1)S(1)}, s32[]{:S(2)}) async-start(s8[8388608]{0:T(1024)(128)(4,1)} %bitcast.186), calls=%async_computation.3 | async-start | bytes 8388608 | tf_op jit(solution)/shard_map/while
  159.3 6.7 %slice-start = ((s8[8388608]{0:T(1024)(128)(4,1)}), s8[4194304]{0:T(1024)(128)(4,1)S(1)}, s32[]{:S(2)}) async-start(s8[8388608]{0:T(1024)(128)(4,1)} %bitcast.186), calls=%async_computation.2 | async-start | bytes 8388608 | tf_op jit(solution)/shard_map/while
  159.3 6.7 %slice-start.1 = ((s8[8388608]{0:T(1024)(128)(4,1)}), s8[4194304]{0:T(1024)(128)(4,1)S(1)}, s32[]{:S(2)}) async-start(s8[8388608]{0:T(1024)(128)(4,1)} %bitcast.186), calls=%async_computation.3 | async-start | bytes 8388608 | tf_op jit(solution)/shard_map/while
  182.2 6.7 %slice-start = ((s8[8388608]{0:T(1024)(128)(4,1)}), s8[4194304]{0:T(1024)(128)(4,1)S(1)}, s32[]{:S(2)}) async-start(s8[8388608]{0:T(1024)(128)(4,1)} %bitcast.186), calls=%async_computation.2 | async-start | bytes 8388608 | tf_op jit(solution)/shard_map/while
  182.2 6.7 %slice-start.1 = ((s8[8388608]{0:T(1024)(128)(4,1)}), s8[4194304]{0:T(1024)(128)(4,1)S(1)}, s32[]{:S(2)}) async-start(s8[8388608]{0:T(1024)(128)(4,1)} %bitcast.186), calls=%async_computation.3 | async-start | bytes 8388608 | tf_op jit(solution)/shard_map/while
  197.3 16.2 %all-to-all-start = ((bf16[2,1024,256]{2,0,1:T(2,128)(2,1)}), bf16[2,1024,256]{2,0,1:T(2,128)(2,1)S(1)}, u32[]{:S(2)}, u32[]{:S(2)}) async-start(bf16[2,1024,256]{2,0,1:T(2,128)(2,1)} %copy.27), calls=%async_computation | async-start | bytes 2097152 | tf_op jit(solution)/shard_map/all_to_all | solution.py:200
Sparse Core Ops, SparseCore 0:
  70.4 52.5 all-gather.1
where the time goes:
time: 227 us; the launch traced here: 226 us
  matrix products  74.6 us (33%)
  blocking collectives  66.1 us (29%)
  other arithmetic  38.5 us (17%)
  local copies, waits for them, and re-layouts  17.8 us (8%)
  between operations  13.7 us (6%)
  loops' own time  9.49 us (4%)
  starting transfers between devices  6.28 us (3%)
    psum x1, blocking collectives, shards(): lax.psum((jnp.dot(active, w_shift, preferred_element_type=jnp.float32), j...  21.3 us
    reduce_sum x4, other arithmetic, attend(): far_exp.sum(-1, keepdims=True)  21 us
    dot_general x4, matrix products, attend(): jnp.einsum('qgrd,kgd->grqk', q_rows, far_keys, preferred_element_type=jnp...  18.3 us
    all_gather x1, blocking collectives, shards(): lax.all_gather(jnp.concatenate([ctx_keys, ctx_values], axis=-1), 'sp', ax...  15.8 us
    all_gather x1, blocking collectives, shards(): lax.all_gather(gate_part, 'tp', axis=1, tiled=True)  12.7 us
    another operation x1, loops' own time, shards(): lax.map(attend, jnp.arange(samples * blocks, dtype=jnp.int32))  9.49 us
    dot_general x4, matrix products, attend(): jnp.einsum('grqk,kgd->qgrd', (far_exp / normaliser).astype(jnp.bfloat16),...  8.49 us
    all_gather x1, blocking collectives, shards(): lax.all_gather(shift_part, 'tp', axis=1, tiled=True)  8.18 us
  transfers between devices with their start and end apart: 4, of which 0 were waited for; matrix products, arithmetic and copies ran while one was open for 45% of the time, Pallas kernels for 0%

commit v1 on v0

--- a/solution.py
+++ b/solution.py
@@ -9,6 +9,23 @@
 epsilon = 1e-06
 rope_base = 10000.0
 masked_value = -1e30
+
+
+def laid_out(blocks, dim):
+    shape = list(blocks.shape[1:])
+    shape[dim] *= blocks.shape[0]
+    return jnp.moveaxis(blocks, 0, dim).reshape(shape)
+
+
+def collect(shard, axis, dim):
+    devices = lax.axis_size(axis)
+    right = [(i, (i + 1) % devices) for i in range(devices)]
+    blocks = [shard]
+    while len(blocks) < devices:
+        blocks.append(lax.ppermute(blocks[-1], axis, right))
+    mine = lax.axis_index(axis)
+    blocks = jnp.stack(blocks)[(mine - jnp.arange(devices)) % devices]
+    return laid_out(blocks, dim)
 
 
 def with_halo(cells, sides, width):
@@ -126,9 +143,7 @@
     ctx_values = jnp.einsum(
         "snd,dc->snc", ctx_hidden, w_value, preferred_element_type=jnp.float32
     ).astype(jnp.bfloat16)
-    context_pairs = lax.all_gather(
-        jnp.concatenate([ctx_keys, ctx_values], axis=-1), "sp", axis=1, tiled=True
-    )
+    context_pairs = collect(jnp.concatenate([ctx_keys, ctx_values], axis=-1), "sp", 1)
     block_rows = min(512, tokens)
     blocks = tokens // block_rows
     span_rows = block_rows + 2 * WINDOW

time: 227 us -> 225 us (level)
  blocking collectives: 66.1 us -> 50.3 us
  waiting for transfers between devices: 0.05 us -> 11.4 us
  starting transfers between devices: 6.28 us -> 10.2 us
  matrix products: 74.6 us -> 71.2 us
    all_gather x1 -> x0, blocking collectives: 15.8 us -> none  [shards(): lax.all_gather(jnp.concatenate([ctx_keys, ctx_values], axis=-1), 'sp', ax...]
    ppermute x0 -> x3, waiting for transfers between devices: none -> 11.4 us  [collect(): blocks.append(lax.ppermute(blocks[-1], axis, right))]
    ppermute x0 -> x3, starting transfers between devices: none -> 4.13 us  [collect(): blocks.append(lax.ppermute(blocks[-1], axis, right))]
  transfers between devices with their start and end apart: 4 -> 7, of which waited for: 0 -> 2; matrix products, arithmetic and copies ran while one was open for 45% -> 44% of each run, Pallas kernels for 0% -> 0%
where the time goes in v1:
time: 225 us; the launch traced here: 224 us
  matrix products  71.2 us (32%)
  blocking collectives  50.3 us (22%)
  other arithmetic  37 us (16%)
  local copies, waits for them, and re-layouts  19.4 us (9%)
  between operations  13.7 us (6%)
  waiting for transfers between devices  11.4 us (5%)
  loops' own time  10.7 us (5%)
  starting transfers between devices  10.2 us (5%)
    psum x1, blocking collectives, shards(): lax.psum((jnp.dot(active, w_shift, preferred_element_type=jnp.float32), j...  21.3 us
    reduce_sum x4, other arithmetic, attend(): far_exp.sum(-1, keepdims=True)  21 us
    dot_general x4, matrix products, attend(): jnp.einsum('qgrd,kgd->grqk', q_rows, far_keys, preferred_element_type=jnp...  18.3 us
    all_gather x1, blocking collectives, shards(): lax.all_gather(gate_part, 'tp', axis=1, tiled=True)  12.7 us
    ppermute x3, waiting for transfers between devices, collect(): blocks.append(lax.ppermute(blocks[-1], axis, right))  11.4 us
    another operation x1, loops' own time, shards(): lax.map(attend, jnp.arange(samples * blocks, dtype=jnp.int32))  10.7 us
    dot_general x4, matrix products, attend(): jnp.einsum('grqk,kgd->qgrd', (far_exp / normaliser).astype(jnp.bfloat16),...  8.49 us
    all_gather x1, blocking collectives, shards(): lax.all_gather(shift_part, 'tp', axis=1, tiled=True)  8.18 us
  transfers between devices with their start and end apart: 7, of which 2 were waited for; matrix products, arithmetic and copies ran while one was open for 44% of the time, Pallas kernels for 0%

profile of v1, /device:TPU:0, one launch (start us, length us, event | category | flops | bytes accessed | tf_op | source)
XLA Modules:
  0.0 223.9 jit_solution(14824014929606318940)
XLA Ops:
  11.1 21.3 %all-reduce = (f32[3,512]{1,0:T(4,128)S(1)}, f32[3,512]{1,0:T(4,128)S(1)}, f32[3,512]{1,0:T(4,128)}) all-reduce(f32[3,512]{1,0:T(4,128)S(1)} %fusion.72, f32[3,512]{1,0:T(4,128)S(1)} %fusion.74, f32[3,512]{1,0:T(4,128)S(1)} %fusion.76), channel_id=1, replica_groups=mesh['sp'=4,'tp'=4,'dp'=2] {'sp'}, use_global_device_ids=true, to_apply=%region_3.4 | all-reduce | flops 4608 | bytes 36864 | tf_op jit(solution)/shard_map/psum | solution.py:100
  32.3 8.2 %all_gather.14 = f32[3,2048]{1,0:T(4,128)S(1)} all-gather(f32[3,512]{1,0:T(4,128)S(1)} %get-tuple-element.196), channel_id=1, replica_groups=mesh['sp'=4,'tp'=4,'dp'=2] {'tp'}, dimensions={1}, use_global_device_ids=true | all-gather | bytes 30720 | tf_op jit(solution)/shard_map/all_gather | solution.py:109
  40.5 8.2 %all_gather.13 = f32[3,2048]{1,0:T(4,128)S(1)} all-gather(f32[3,512]{1,0:T(4,128)S(1)} %get-tuple-element.197), channel_id=1, replica_groups=mesh['sp'=4,'tp'=4,'dp'=2] {'tp'}, dimensions={1}, use_global_device_ids=true | all-gather | bytes 30720 | tf_op jit(solution)/shard_map/all_gather | solution.py:110
  48.7 5.1 %fusion.26 = f32[2,1024]{1,0:T(2,128)S(1)} fusion(bf16[2,1024,2048]{2,1,0:T(8,128)(2,1)} %param.16), kind=kLoop, calls=%fused_computation.45 | loop fusion | flops 12580864 | bytes 8396800 | tf_op jit(solution)/shard_map/reduce_sum | solution.py:50
  54.4 6.0 %convolution_bitcast_fusion = f32[2,1024,1,64]{1,3,0,2:T(8,128)S(1)} fusion(bf16[2,1024,2048]{2,1,0:T(8,128)(2,1)} %param.16, f32[2,2048]{1,0:T(2,128)S(1)} %slice.76, f32[2,2048]{1,0:T(2,128)S(1)} %slice_add_fusion, f32[2048]{0:T(1024)S(1)} %copy-done.7, f32[2,1024]{1,0:T(2,128)S(1)} %add_rsqrt_fusion, bf16[2048,64]{0,1:T(8,128)(2,1)S(1)} %copy-done.6), kind=kOutput, calls=%fused_computation.60 | convolution fusion | flops 562036736 | bytes 9224192 | tf_op jit(solution)/shard_map/snd,dc->snc/dot_general | solution.py:129
  60.6 7.1 %fusion.40 = bf16[2,1024,128]{1,2,0:T(8,128)(2,1)S(1)} fusion(bf16[2,1024,128]{1,2,0:T(8,128)(2,1)S(1)} %fusion.59, bf16[2,1024,2048]{2,1,0:T(8,128)(2,1)} %param.16, f32[2,2048]{1,0:T(2,128)S(1)} %slice.76, f32[2,2048]{1,0:T(2,128)S(1)} %slice_add_fusion, f32[2048]{0:T(1024)S(1)} %copy-done.7, f32[2,1024]{1,0:T(2,128)S(1)} %add_rsqrt_fusion, ...), kind=kOutput, calls=%fused_computation.62 | convolution fusion | flops 562167808 | bytes 8962048 | tf_op jit(solution)/shard_map/snd,dc->snc/dot_general | solution.py:134
  72.9 2.9 %collective-permute-start.2 = (bf16[2,256,128]{1,2,0:T(8,128)(2,1)S(1)}, bf16[2,256,128]{1,2,0:T(8,128)(2,1)S(1)}, u32[]{:S(2)}, u32[]{:S(2)}) collective-permute-start(bf16[2,256,128]{1,2,0:T(8,128)(2,1)S(1)} %get-tuple-element.212), channel_id=1, source_target_pairs={{0,8},{8,16},{16,24},{24,0},{1,9},{9,17},{17,25},{25,1},{2,10},{10... | collective-permute-start | bytes 393224 | tf_op jit(solution)/shard_map/ppermute | solution.py:25
  75.8 6.3 %fusion.43 = f32[2,1024,256]{1,2,0:T(8,128)S(1)} fusion(bf16[2048,256]{1,0:T(8,128)(2,1)S(1)} %copy-done, bf16[2,1024,2048]{2,1,0:T(8,128)(2,1)} %param.16, f32[2,2048]{1,0:T(2,128)S(1)} %slice.76, f32[2,2048]{1,0:T(2,128)S(1)} %slice_add_fusion, f32[2048]{0:T(1024)S(1)} %copy-done.7, f32[2,1024]{1,0:T(2,128)S(1)} %add_rsqrt_fusion), kind=kOutput, calls=%fused_computation.66 | convolution fusion | flops 2172649472 | bytes 11583488 | tf_op jit(solution)/shard_map/snd,dc->snc/dot_general | solution.py:123
  83.9 5.5 %collective-permute-done.3 = bf16[2,256,128]{1,2,0:T(8,128)(2,1)S(1)} collective-permute-done((bf16[2,256,128]{1,2,0:T(8,128)(2,1)S(1)}, bf16[2,256,128]{1,2,0:T(8,128)(2,1)S(1)}, u32[]{:S(2)}, u32[]{:S(2)}) %collective-permute-start.3) | collective-permute-done | bytes 131104 | tf_op jit(solution)/shard_map/ppermute | solution.py:25
  90.4 5.8 %collective-permute-done.4 = bf16[2,256,128]{1,2,0:T(8,128)(2,1)S(1)} collective-permute-done((bf16[2,256,128]{1,2,0:T(8,128)(2,1)S(1)}, bf16[2,256,128]{1,2,0:T(8,128)(2,1)S(1)}, u32[]{:S(2)}, u32[]{:S(2)}) %collective-permute-start.4) | collective-permute-done | bytes 131104 | tf_op jit(solution)/shard_map/ppermute | solution.py:25
  97.7 93.7 %while.13 = (s32[]{:T(128)}, bf16[4,512,256]{2,1,0:T(8,128)(2,1)}, s32[4]{0:T(128)}, bf16[2,1280,128]{1,2,0:T(8,128)(2,1)}, s32[]{:T(128)}, /*index=5*/bf16[2,10...) while((s32[]{:T(128)}, bf16[4,512,256]{2,1,0:T(8,128)(2,1)}, ...), condition=%wide.region_10.11_spmd, body=%wide.region_5.10_spmd.sunk | while | flops 985405696 | bytes 75716256 | solution.py:212
  101.8 4.6 %bitcast_reduce_fusion.2 = (f32[4,512]{1,0:T(4,128)S(1)}, f32[1024,512,4]{1,0,2:T(8,128)}) fusion(f32[4]{0:T(128)S(1)} %bitcast.209, bf16[2,1024,4,64]{1,3,2,0:T(8,128)(2,1)S(1)} %get-tuple-element.323, s32[]{:T(128)S(6)} %select_n.154, s32[]{:T(128)S(6)} %select_n.157, bf16[1024,128]{0,1:T(8,128)(2,1)S(1)} %bitcast.196), kind=kOutput, calls=%fused_computation.2.clone.1 | convolution fusion | flops 274724864 | bytes 8790536 | tf_op jit(solution)/shard_map/while/body/eval_jaxpr/qgrd,kgd->grqk/dot_general | solution.py:183
  109.4 5.2 %fusion.97 = f32[4,512]{1,0:T(4,128)S(1)} fusion(f32[1024,512,4]{1,0,2:T(8,128)} %get-tuple-element.280, f32[4,512]{1,0:T(4,128)S(1)} %maximum_maximum_fusion.2, f32[4]{0:T(128)S(1)} %bitcast.210), kind=kLoop, calls=%fused_computation.6.clone.1 | loop fusion | flops 8386560 | bytes 8405008 | tf_op jit(solution)/shard_map/while/body/eval_jaxpr/reduce_sum | solution.py:195
  116.2 2.1 fusion.98
  118.3 2.0 fusion.99
  125.2 4.6 %bitcast_reduce_fusion.2 = (f32[4,512]{1,0:T(4,128)S(1)}, f32[1024,512,4]{1,0,2:T(8,128)}) fusion(f32[4]{0:T(128)S(1)} %bitcast.209, bf16[2,1024,4,64]{1,3,2,0:T(8,128)(2,1)S(1)} %get-tuple-element.323, s32[]{:T(128)S(6)} %select_n.154, s32[]{:T(128)S(6)} %select_n.157, bf16[1024,128]{0,1:T(8,128)(2,1)S(1)} %bitcast.196), kind=kOutput, calls=%fused_computation.2.clone.1 | convolution fusion | flops 274724864 | bytes 8790536 | tf_op jit(solution)/shard_map/while/body/eval_jaxpr/qgrd,kgd->grqk/dot_general | solution.py:183
  132.8 5.2 %fusion.97 = f32[4,512]{1,0:T(4,128)S(1)} fusion(f32[1024,512,4]{1,0,2:T(8,128)} %get-tuple-element.280, f32[4,512]{1,0:T(4,128)S(1)} %maximum_maximum_fusion.2, f32[4]{0:T(128)S(1)} %bitcast.210), kind=kLoop, calls=%fused_computation.6.clone.1 | loop fusion | flops 8386560 | bytes 8405008 | tf_op jit(solution)/shard_map/while/body/eval_jaxpr/reduce_sum | solution.py:195
  138.1 1.4 fusion.96
  139.6 2.1 fusion.98
  141.7 2.0 fusion.99
  148.6 4.6 %bitcast_reduce_fusion.2 = (f32[4,512]{1,0:T(4,128)S(1)}, f32[1024,512,4]{1,0,2:T(8,128)}) fusion(f32[4]{0:T(128)S(1)} %bitcast.209, bf16[2,1024,4,64]{1,3,2,0:T(8,128)(2,1)S(1)} %get-tuple-element.323, s32[]{:T(128)S(6)} %select_n.154, s32[]{:T(128)S(6)} %select_n.157, bf16[1024,128]{0,1:T(8,128)(2,1)S(1)} %bitcast.196), kind=kOutput, calls=%fused_computation.2.clone.1 | convolution fusion | flops 274724864 | bytes 8790536 | tf_op jit(solution)/shard_map/while/body/eval_jaxpr/qgrd,kgd->grqk/dot_general | solution.py:183
  156.3 5.2 %fusion.97 = f32[4,512]{1,0:T(4,128)S(1)} fusion(f32[1024,512,4]{1,0,2:T(8,128)} %get-tuple-element.280, f32[4,512]{1,0:T(4,128)S(1)} %maximum_maximum_fusion.2, f32[4]{0:T(128)S(1)} %bitcast.210), kind=kLoop, calls=%fused_computation.6.clone.1 | loop fusion | flops 8386560 | bytes 8405008 | tf_op jit(solution)/shard_map/while/body/eval_jaxpr/reduce_sum | solution.py:195
  163.0 2.1 fusion.98
  165.1 2.0 fusion.99
  172.1 4.6 %bitcast_reduce_fusion.2 = (f32[4,512]{1,0:T(4,128)S(1)}, f32[1024,512,4]{1,0,2:T(8,128)}) fusion(f32[4]{0:T(128)S(1)} %bitcast.209, bf16[2,1024,4,64]{1,3,2,0:T(8,128)(2,1)S(1)} %get-tuple-element.323, s32[]{:T(128)S(6)} %select_n.154, s32[]{:T(128)S(6)} %select_n.157, bf16[1024,128]{0,1:T(8,128)(2,1)S(1)} %bitcast.196), kind=kOutput, calls=%fused_computation.2.clone.1 | convolution fusion | flops 274724864 | bytes 8790536 | tf_op jit(solution)/shard_map/while/body/eval_jaxpr/qgrd,kgd->grqk/dot_general | solution.py:183
  179.7 5.2 %fusion.97 = f32[4,512]{1,0:T(4,128)S(1)} fusion(f32[1024,512,4]{1,0,2:T(8,128)} %get-tuple-element.280, f32[4,512]{1,0:T(4,128)S(1)} %maximum_maximum_fusion.2, f32[4]{0:T(128)S(1)} %bitcast.210), kind=kLoop, calls=%fused_computation.6.clone.1 | loop fusion | flops 8386560 | bytes 8405008 | tf_op jit(solution)/shard_map/while/body/eval_jaxpr/reduce_sum | solution.py:195
  186.4 2.1 fusion.98
  188.5 2.0 fusion.99
  191.4 3.3 %copy.31 = bf16[2,1024,256]{2,0,1:T(2,128)(2,1)} copy(bf16[2,1024,256]{2,1,0:T(8,128)(2,1)} %bitcast.203) | data formatting | bytes 2097152 | tf_op jit(solution)/shard_map/reshape | solution.py:212
  194.7 3.5 %all-to-all-start = ((bf16[2,1024,256]{2,0,1:T(2,128)(2,1)}), bf16[2,1024,256]{2,0,1:T(2,128)(2,1)S(1)}, u32[]{:S(2)}, u32[]{:S(2)}) async-start(bf16[2,1024,256]{2,0,1:T(2,128)(2,1)} %copy.31), calls=%async_computation | async-start | bytes 2097152 | tf_op jit(solution)/shard_map/all_to_all | solution.py:215
  198.2 12.7 %all_gather.12 = f32[3,2048]{1,0:T(4,128)S(1)} all-gather(f32[3,512]{1,0:T(4,128)S(1)} %copy-done.4), channel_id=1, replica_groups=mesh['sp'=4,'tp'=4,'dp'=2] {'tp'}, dimensions={1}, use_global_device_ids=true | all-gather | bytes 30720 | tf_op jit(solution)/shard_map/all_gather | solution.py:111
  211.2 5.8 %multiply_convert_fusion = bf16[2,256,2048]{2,1,0:T(8,128)(2,1)} fusion(bf16[2,256,1024]{2,1,0:T(8,128)(2,1)S(1)} %bitcast.204, bf16[1024,2048]{1,0:T(8,128)(2,1)} %all-gather.2.cloned.1.call-done, f32[2,2048]{1,0:T(2,128)S(1)} %slice.74), kind=kOutput, calls=%fused_computation.59 | convolution fusion | flops 2149580800 | bytes 7356416 | tf_op jit(solution)/shard_map/snc,cd->snd/dot_general | solution.py:216
  (137 shorter events, 40.6 us)
Async XLA Ops:
  6.5 69.3 %copy-start = (bf16[2048,256]{1,0:T(8,128)(2,1)S(1)}, bf16[2048,256]{1,0:T(8,128)(2,1)}, u32[]{:S(2)}) copy-start(bf16[2048,256]{1,0:T(8,128)(2,1)} %param.24) | copy-start | bytes 3145732
  6.5 47.8 %copy-start.7 = (f32[2048]{0:T(1024)S(1)}, f32[2048]{0:T(1024)}, u32[]{:S(2)}) copy-start(f32[2048]{0:T(1024)} %param.20) | copy-start | bytes 24580
  6.5 47.9 %copy-start.6 = (bf16[2048,64]{0,1:T(8,128)(2,1)S(1)}, bf16[2048,64]{0,1:T(8,128)(2,1)}, u32[]{:S(2)}) copy-start(bf16[2048,64]{0,1:T(8,128)(2,1)} %param.25) | copy-start | bytes 786436
  6.5 204.7 %all-gather.2.cloned.1.call-start = ((), (), s32[]{:S(2)}) async-start(), calls=%async_computation.1 | async-start | bytes 5242880 | tf_op jit(solution)/shard_map/all_gather | solution.py:219
  54.4 6.1 %copy-start.5 = (bf16[2048,64]{0,1:T(8,128)(2,1)S(1)}, bf16[2048,64]{0,1:T(8,128)(2,1)}, u32[]{:S(2)}) copy-start(bf16[2048,64]{0,1:T(8,128)(2,1)} %param.26) | copy-start | bytes 786436
  60.5 9.8 %copy-start.1 = (bf16[2,256,2048]{2,1,0:T(8,128)(2,1)S(1)}, bf16[2,256,2048]{2,1,0:T(8,128)(2,1)}, u32[]{:S(2)}) copy-start(bf16[2,256,2048]{2,1,0:T(8,128)(2,1)} %param.17) | copy-start | bytes 6291460
  67.7 21.8 %collective-permute-start = (bf16[2,128,128]{1,2,0:T(8,128)(2,1)S(1)}, bf16[2,128,128]{1,2,0:T(8,128)(2,1)S(1)}, u32[]{:S(2)}, u32[]{:S(2)}) collective-permute-start(bf16[2,128,128]{1,2,0:T(8,128)(2,1)S(1)} %get-tuple-element.209), channel_id=1, source_target_pairs={{0,8},{8,16},{16,24},{1,9},{9,17},{17,25},{2,10},{10,18},{18,26},{... | collective-permute-start | bytes 196616 | tf_op jit(solution)/shard_map/ppermute | solution.py:39
  69.0 20.5 %collective-permute-start.1 = (bf16[2,128,128]{1,2,0:T(8,128)(2,1)S(1)}, bf16[2,128,128]{1,2,0:T(8,128)(2,1)S(1)}, u32[]{:S(2)}, u32[]{:S(2)}) collective-permute-start(bf16[2,128,128]{1,2,0:T(8,128)(2,1)S(1)} %get-tuple-element.210), channel_id=1, source_target_pairs={{8,0},{16,8},{24,16},{9,1},{17,9},{25,17},{10,2},{18,10},{26,18},{... | collective-permute-start | bytes 196616 | tf_op jit(solution)/shard_map/ppermute | solution.py:41
  72.9 9.7 %collective-permute-start.2 = (bf16[2,256,128]{1,2,0:T(8,128)(2,1)S(1)}, bf16[2,256,128]{1,2,0:T(8,128)(2,1)S(1)}, u32[]{:S(2)}, u32[]{:S(2)}) collective-permute-start(bf16[2,256,128]{1,2,0:T(8,128)(2,1)S(1)} %get-tuple-element.212), channel_id=1, source_target_pairs={{0,8},{8,16},{16,24},{24,0},{1,9},{9,17},{17,25},{25,1},{2,10},{10... | collective-permute-start | bytes 393224 | tf_op jit(solution)/shard_map/ppermute | solution.py:25
  82.1 15.6 %copy-start.2 = (f32[4]{0:T(128)S(1)}, f32[4]{0:T(128)}, u32[]{:S(2)}) copy-start(f32[4]{0:T(128)} %param.29) | copy-start | bytes 52
  82.2 15.6 %copy-start.3 = (f32[4]{0:T(128)S(1)}, f32[4]{0:T(128)}, u32[]{:S(2)}) copy-start(f32[4]{0:T(128)} %param.28) | copy-start | bytes 52
  82.6 6.8 %collective-permute-start.3 = (bf16[2,256,128]{1,2,0:T(8,128)(2,1)S(1)}, bf16[2,256,128]{1,2,0:T(8,128)(2,1)S(1)}, u32[]{:S(2)}, u32[]{:S(2)}) collective-permute-start(bf16[2,256,128]{1,2,0:T(8,128)(2,1)S(1)} %collective-permute-done.2), channel_id=1, source_target_pairs={{0,8},{8,16},{16,24},{24,0},{1,9},{9,17},{17,25},{25,1},{2,10},{10... | collective-permute-start | bytes 393224 | tf_op jit(solution)/shard_map/ppermute | solution.py:25
  89.5 6.8 %collective-permute-start.4 = (bf16[2,256,128]{1,2,0:T(8,128)(2,1)S(1)}, bf16[2,256,128]{1,2,0:T(8,128)(2,1)S(1)}, u32[]{:S(2)}, u32[]{:S(2)}) collective-permute-start(bf16[2,256,128]{1,2,0:T(8,128)(2,1)S(1)} %collective-permute-done.3), channel_id=1, source_target_pairs={{0,8},{8,16},{16,24},{24,0},{1,9},{9,17},{17,25},{25,1},{2,10},{10... | collective-permute-start | bytes 393224 | tf_op jit(solution)/shard_map/ppermute | solution.py:25
  97.7 100.5 %copy-start.4 = (f32[3,512]{1,0:T(4,128)S(1)}, f32[3,512]{1,0:T(4,128)}, u32[]{:S(2)}) copy-start(f32[3,512]{1,0:T(4,128)} %get-tuple-element.198) | copy-start | bytes 18436
  109.4 6.7 %slice-start = ((s8[8388608]{0:T(1024)(128)(4,1)}), s8[4194304]{0:T(1024)(128)(4,1)S(1)}, s32[]{:S(2)}) async-start(s8[8388608]{0:T(1024)(128)(4,1)} %bitcast.194), calls=%async_computation.2 | async-start | bytes 8388608 | tf_op jit(solution)/shard_map/while
  109.4 6.7 %slice-start.1 = ((s8[8388608]{0:T(1024)(128)(4,1)}), s8[4194304]{0:T(1024)(128)(4,1)S(1)}, s32[]{:S(2)}) async-start(s8[8388608]{0:T(1024)(128)(4,1)} %bitcast.194), calls=%async_computation.3 | async-start | bytes 8388608 | tf_op jit(solution)/shard_map/while
  132.8 6.7 %slice-start = ((s8[8388608]{0:T(1024)(128)(4,1)}), s8[4194304]{0:T(1024)(128)(4,1)S(1)}, s32[]{:S(2)}) async-start(s8[8388608]{0:T(1024)(128)(4,1)} %bitcast.194), calls=%async_computation.2 | async-start | bytes 8388608 | tf_op jit(solution)/shard_map/while
  132.8 6.7 %slice-start.1 = ((s8[8388608]{0:T(1024)(128)(4,1)}), s8[4194304]{0:T(1024)(128)(4,1)S(1)}, s32[]{:S(2)}) async-start(s8[8388608]{0:T(1024)(128)(4,1)} %bitcast.194), calls=%async_computation.3 | async-start | bytes 8388608 | tf_op jit(solution)/shard_map/while
  156.3 6.7 %slice-start = ((s8[8388608]{0:T(1024)(128)(4,1)}), s8[4194304]{0:T(1024)(128)(4,1)S(1)}, s32[]{:S(2)}) async-start(s8[8388608]{0:T(1024)(128)(4,1)} %bitcast.194), calls=%async_computation.2 | async-start | bytes 8388608 | tf_op jit(solution)/shard_map/while
  156.3 6.7 %slice-start.1 = ((s8[8388608]{0:T(1024)(128)(4,1)}), s8[4194304]{0:T(1024)(128)(4,1)S(1)}, s32[]{:S(2)}) async-start(s8[8388608]{0:T(1024)(128)(4,1)} %bitcast.194), calls=%async_computation.3 | async-start | bytes 8388608 | tf_op jit(solution)/shard_map/while
  179.7 6.7 %slice-start = ((s8[8388608]{0:T(1024)(128)(4,1)}), s8[4194304]{0:T(1024)(128)(4,1)S(1)}, s32[]{:S(2)}) async-start(s8[8388608]{0:T(1024)(128)(4,1)} %bitcast.194), calls=%async_computation.2 | async-start | bytes 8388608 | tf_op jit(solution)/shard_map/while
  179.7 6.7 %slice-start.1 = ((s8[8388608]{0:T(1024)(128)(4,1)}), s8[4194304]{0:T(1024)(128)(4,1)S(1)}, s32[]{:S(2)}) async-start(s8[8388608]{0:T(1024)(128)(4,1)} %bitcast.194), calls=%async_computation.3 | async-start | bytes 8388608 | tf_op jit(solution)/shard_map/while
  194.7 16.2 %all-to-all-start = ((bf16[2,1024,256]{2,0,1:T(2,128)(2,1)}), bf16[2,1024,256]{2,0,1:T(2,128)(2,1)S(1)}, u32[]{:S(2)}, u32[]{:S(2)}) async-start(bf16[2,1024,256]{2,0,1:T(2,128)(2,1)} %copy.31), calls=%async_computation | async-start | bytes 2097152 | tf_op jit(solution)/shard_map/all_to_all | solution.py:215
Sparse Core Ops, SparseCore 0:
  76.0 50.4 all-gather.1
